TPU v7x, 128 devices: a whole 4x4x4 slice. The times are simulated.
128 devices in a mesh: kv: 16 (over z, y), tp: 8 (over x, core).
Axes of the slice: x: 4, y: 4, z: 4, core: 2. Of those that a mesh axis runs over, the one named last changes fastest.
Arguments:
- block_in: bfloat16 [128, 4096], P(None, ('kv', 'tp')), may hold values from -30 to 30
- before_gain: bfloat16 [4096], P('kv'), may hold values from 0.099609375 to 1.8984375
- before_gate: bfloat16 [4096, 11264], P('kv', 'tp'), may hold values from -0.09375 to 0.09375
- before_up: bfloat16 [4096, 11264], P('kv', 'tp'), may hold values from -0.09375 to 0.09375
- before_down: bfloat16 [11264, 4096], P('tp', 'kv'), may hold values from -0.0546875 to 0.0546875
- mix_gain: bfloat16 [4096], P('kv'), may hold values from 0.099609375 to 1.8984375
- input_gate: bfloat16 [4096, 8192], P('kv', 'tp'), may hold values from -0.09375 to 0.09375
- input_value: bfloat16 [4096, 8192], P('kv', 'tp'), may hold values from -0.09375 to 0.09375
- input_write: bfloat16 [4096, 2048], P('kv', 'tp'), may hold values from -0.09375 to 0.09375
- input_read: bfloat16 [4096, 2048], P('kv', 'tp'), may hold values from -0.09375 to 0.09375
- input_step: bfloat16 [4096, 128], P('kv', 'tp'), may hold values from -0.09375 to 0.09375
- step_bias: float32 [128], P('tp'), may hold values from -3 to 0
- decay_log: float32 [128], P('tp'), may hold values from -1 to 1.4
- skip_gain: float32 [128], P('tp'), may hold values from 0.5 to 2
- value_taps: bfloat16 [4, 8192], P(None, 'tp'), may hold values from -3 to 3
- write_taps: bfloat16 [4, 2048], P(None, 'tp'), may hold values from -3 to 3
- read_taps: bfloat16 [4, 2048], P(None, 'tp'), may hold values from -3 to 3
- value_window: bfloat16 [128, 3, 8192], P('kv', None, 'tp'), may hold values from -6 to 6
- write_window: bfloat16 [128, 3, 2048], P('kv', None, 'tp'), may hold values from -6 to 6
- read_window: bfloat16 [128, 3, 2048], P('kv', None, 'tp'), may hold values from -6 to 6
- scan_state: float32 [128, 128, 64, 128], P('kv', 'tp'), may hold values from -2 to 2
- group_gain: bfloat16 [8192], P('tp'), may hold values from 0.099609375 to 1.8984375
- mixer_out: bfloat16 [8192, 4096], P('tp', 'kv'), may hold values from -0.0625 to 0.0625
- after_gain: bfloat16 [4096], P('kv'), may hold values from 0.099609375 to 1.8984375
- after_gate: bfloat16 [4096, 11264], P('kv', 'tp'), may hold values from -0.09375 to 0.09375
- after_up: bfloat16 [4096, 11264], P('kv', 'tp'), may hold values from -0.09375 to 0.09375
- after_down: bfloat16 [11264, 4096], P('tp', 'kv'), may hold values from -0.0546875 to 0.0546875
Outputs:
- block_out: bfloat16 [128, 4096], P(None, ('kv', 'tp'))
- state_next: float32 [128, 128, 64, 128], P('kv', 'tp')
- value_next: bfloat16 [128, 3, 8192], P('kv', None, 'tp')
- write_next: bfloat16 [128, 3, 2048], P('kv', None, 'tp')
- read_next: bfloat16 [128, 3, 2048], P('kv', None, 'tp')
All inputs are finite; a program needn't handle non-finite values.
Results may differ from a plain program's by a relative error of at most 0.0085.
Values may be sent and summed in bfloat16 or wider, within the bound.
A program may use at most 64 MiB of HBM per device.

v0:
```python
import jax
import jax.numpy as jnp
from jax import lax
from jax.sharding import PartitionSpec as P

D = 4096
HEAD_DIM = 64
STATE = 128
EPS = 1e-06


def copy_for_each(shard, axis):
    copies = jnp.broadcast_to(shard, (lax.axis_size(axis), *shard.shape))
    return lax.all_to_all(copies, axis, split_axis=0, concat_axis=0, tiled=True)


def in_order(blocks, dim):
    shape = list(blocks.shape[1:])
    shape[dim] *= blocks.shape[0]
    return jnp.moveaxis(blocks, 0, dim).reshape(shape)


def gather_directly(shard, axis, dim):
    blocks = copy_for_each(shard, axis)
    return in_order(blocks, dim)


def in_blocks(shard, dim, length):
    before, after = (shard.shape[:dim], shard.shape[dim + 1 :])
    return jnp.moveaxis(shard.reshape(*before, length, -1, *after), dim, 0)


def sent_and_summed(shard, axis, dim):
    length = lax.axis_size(axis)
    blocks = lax.all_to_all(in_blocks(shard, dim, length), axis, 0, 0, tiled=True)
    return jnp.sum(blocks, axis=0)


def sum_at_owner(shard, axis, dim):
    blocks = in_blocks(shard, dim, lax.axis_size(axis))
    arrived = lax.all_to_all(blocks, axis, split_axis=0, concat_axis=0, tiled=True)
    return arrived.astype(jnp.float32).sum(axis=0)


def side_by_side(arrays, axis, dim, along):
    ends, at = ([], 0)
    for a in arrays[:-1]:
        at += a.shape[along]
        ends.append(at)
    both = jnp.concatenate(arrays, axis=along)
    return tuple(jnp.split(sum_at_owner(both, axis, dim), ends, axis=along))


def in_one_piece(arrays, axis, dim, along):
    columns = [a.reshape(*a.shape[:along], -1) for a in arrays]
    both = jnp.concatenate(columns, axis=along)
    result, at, gathered = (sent_and_summed(both, axis, dim), 0, [])
    for a, column in zip(arrays, columns):
        share = result[..., at : at + column.shape[along]]
        gathered.append(share.reshape(*share.shape[:along], *a.shape[along:]))
        at += column.shape[along]
    return tuple(gathered)


def lifted_rows(current, gain_vec):
    gathered = gather_directly(current, "tp", 1)
    widened = gathered.astype(jnp.float32)
    squares = jnp.sum(widened * widened, axis=1)
    lifted = (widened * gain_vec.astype(jnp.float32)[None, :]).astype(jnp.bfloat16)
    return (lifted, squares)


def column_sums(partial_terms):
    return sent_and_summed(partial_terms, "tp", 1)


def half_channel(current, gain_vec, gate_weight, up_weight, down_weight):
    lifted, squares = lifted_rows(current, gain_vec)
    gate_part = jnp.dot(lifted, gate_weight, preferred_element_type=jnp.float32)
    up_part = jnp.dot(lifted, up_weight, preferred_element_type=jnp.float32)
    spread_squares = jnp.broadcast_to(squares[:, None], (squares.shape[0], lax.axis_size("kv")))
    gate_sum, up_sum, totals = (
        *side_by_side((gate_part.astype(jnp.bfloat16), up_part.astype(jnp.bfloat16)), "kv", 1, 0),
        sum_at_owner(spread_squares.astype(jnp.bfloat16), "kv", 1),
    )
    row_scale = lax.rsqrt(totals / D + EPS)
    hidden_share = (jax.nn.silu(gate_sum * row_scale) * (up_sum * row_scale)).astype(jnp.bfloat16)
    down_sum = jnp.dot(
        gather_directly(hidden_share, "kv", 1), down_weight, preferred_element_type=jnp.float32
    )
    returned = column_sums(down_sum)
    return (current.astype(jnp.float32) + 0.5 * returned).astype(jnp.bfloat16)


def short_conv(window_state, fresh, taps):
    window = jnp.concatenate([window_state, fresh[:, None, :]], axis=1)
    conv_sum = jnp.sum(window.astype(jnp.float32) * taps.astype(jnp.float32)[None], axis=1)
    return (jax.nn.silu(conv_sum), window[:, 1:])


def spread_groups(vectors, heads):
    count = vectors.shape[0]
    groups = vectors.shape[1] // STATE
    shaped = vectors.reshape(count, groups, 1, STATE)
    return jnp.broadcast_to(shaped, (count, groups, heads // groups, STATE)).reshape(
        count, heads, STATE
    )


def state_update(
    gate_rows,
    value_conv,
    write_conv,
    read_conv,
    step_raw,
    step_bias,
    decay_log,
    skip_gain,
    scan_state,
):
    count = value_conv.shape[0]
    heads = step_bias.shape[0]
    step_size = jax.nn.softplus(step_raw + step_bias[None, :])
    decay = jnp.exp(-step_size * jnp.exp(decay_log)[None, :])
    value_heads = value_conv.reshape(count, heads, HEAD_DIM)
    write_heads = spread_groups(write_conv, heads)
    read_heads = spread_groups(read_conv, heads)
    state_next = (
        decay[:, :, None, None] * scan_state
        + (step_size[:, :, None] * value_heads)[:, :, :, None] * write_heads[:, :, None, :]
    )
    readout = (
        jnp.sum(state_next * read_heads[:, :, None, :], axis=3)
        + skip_gain[None, :, None] * value_heads
    )
    gated = readout.reshape(count, heads * HEAD_DIM) * jax.nn.silu(gate_rows.astype(jnp.float32))
    groups = write_conv.shape[1] // STATE
    grouped = gated.reshape(count, groups, heads * HEAD_DIM // groups)
    grouped = grouped * lax.rsqrt(jnp.mean(grouped * grouped, axis=2, keepdims=True) + EPS)
    return (grouped.reshape(count, heads * HEAD_DIM), state_next)


def local(
    block_in,
    before_gain,
    before_gate,
    before_up,
    before_down,
    mix_gain,
    input_gate,
    input_value,
    input_write,
    input_read,
    input_step,
    step_bias,
    decay_log,
    skip_gain,
    value_taps,
    write_taps,
    read_taps,
    value_window,
    write_window,
    read_window,
    scan_state,
    group_gain,
    mixer_out,
    after_gain,
    after_gate,
    after_up,
    after_down,
):
    first_out = half_channel(block_in, before_gain, before_gate, before_up, before_down)
    lifted, squares = lifted_rows(first_out, mix_gain)
    gate_part = jnp.dot(lifted, input_gate, preferred_element_type=jnp.float32)
    value_part = jnp.dot(lifted, input_value, preferred_element_type=jnp.float32)
    write_part = jnp.dot(lifted, input_write, preferred_element_type=jnp.float32)
    read_part = jnp.dot(lifted, input_read, preferred_element_type=jnp.float32)
    step_part = jnp.dot(lifted, input_step, preferred_element_type=jnp.float32)
    gate_sum, value_sum, write_sum, read_sum, step_sum, totals = in_one_piece(
        (gate_part, value_part, write_part, read_part, step_part, squares), "kv", 0, 1
    )
    mix_scale = lax.rsqrt(totals / D + EPS)[:, None]
    gate_rows = (gate_sum * mix_scale).astype(jnp.bfloat16)
    value_fresh = (value_sum * mix_scale).astype(jnp.bfloat16)
    write_fresh = (write_sum * mix_scale).astype(jnp.bfloat16)
    read_fresh = (read_sum * mix_scale).astype(jnp.bfloat16)
    step_raw = step_sum * mix_scale
    value_conv, value_next = short_conv(value_window, value_fresh, value_taps)
    write_conv, write_next = short_conv(write_window, write_fresh, write_taps)
    read_conv, read_next = short_conv(read_window, read_fresh, read_taps)
    normed, state_next = state_update(
        gate_rows,
        value_conv,
        write_conv,
        read_conv,
        step_raw,
        step_bias,
        decay_log,
        skip_gain,
        scan_state,
    )
    mixer_rows = (normed * group_gain.astype(jnp.float32)[None, :]).astype(jnp.bfloat16)
    back_part = jnp.dot(
        lax.all_gather(mixer_rows, "kv", axis=0, tiled=True),
        mixer_out,
        preferred_element_type=jnp.float32,
    )
    returned = column_sums(back_part)
    middle = (first_out.astype(jnp.float32) + returned).astype(jnp.bfloat16)
    block_out = half_channel(middle, after_gain, after_gate, after_up, after_down)
    return (block_out, state_next, value_next, write_next, read_next)


def solution(mesh):
    placed = (
        P(None, ("kv", "tp")),
        P("kv"),
        P("kv", "tp"),
        P("kv", "tp"),
        P("tp", "kv"),
        P("kv"),
        P("kv", "tp"),
        P("kv", "tp"),
        P("kv", "tp"),
        P("kv", "tp"),
        P("kv", "tp"),
        P("tp"),
        P("tp"),
        P("tp"),
        P(None, "tp"),
        P(None, "tp"),
        P(None, "tp"),
        P("kv", None, "tp"),
        P("kv", None, "tp"),
        P("kv", None, "tp"),
        P("kv", "tp", None, None),
        P("tp"),
        P("tp", "kv"),
        P("kv"),
        P("kv", "tp"),
        P("kv", "tp"),
        P("tp", "kv"),
    )
    return jax.shard_map(
        local,
        mesh=mesh,
        in_specs=placed,
        out_specs=(
            P(None, ("kv", "tp")),
            P("kv", "tp", None, None),
            P("kv", None, "tp"),
            P("kv", None, "tp"),
            P("kv", None, "tp"),
        ),
        check_vma=False,
    )
```

profile of v0, /device:TPU:1, one launch (start us, length us, event | category | flops | bytes accessed | tf_op | source)
XLA Modules:
  0.0 210.5 jit_solution(9722446378386201120)
XLA Ops:
  2.1 5.8 %all-to-all-start = ((bf16[8,128,32]{1,2,0:T(8,128)(2,1)}), bf16[8,128,32]{1,2,0:T(8,128)(2,1)S(1)}, u32[]{:S(2)}, u32[]{:S(2)}) async-start(bf16[8,128,32]{1,2,0:T(8,128)(2,1)} %broadcast_in_dim.20), calls=%async_computation | async-start | bytes 131072 | tf_op jit(solution)/shard_map/all_to_all | solution.py:14
  8.5 4.2 %all-to-all-done = bf16[8,128,32]{1,2,0:T(8,128)(2,1)S(1)} async-done(((bf16[8,128,32]{1,2,0:T(8,128)(2,1)}), bf16[8,128,32]{1,2,0:T(8,128)(2,1)S(1)}, u32[]{:S(2)}, u32[]{:S(2)}) %all-to-all-start) | async-done | bytes 65568 | tf_op jit(solution)/shard_map/all_to_all | solution.py:14
  15.2 7.8 %all-to-all-start.2 = ((bf16[16,128,1]{1,2,0:T(2,128)(2,1)}), bf16[16,128,1]{1,2,0:T(2,128)(2,1)S(1)}, u32[]{:S(2)}, u32[]{:S(2)}) async-start(bf16[16,128,1]{1,2,0:T(2,128)(2,1)} %transpose.92), calls=%async_computation.2 | async-start | bytes 16384 | tf_op jit(solution)/shard_map/all_to_all | solution.py:41
  24.2 5.1 %all-to-all-done.2 = bf16[16,128,1]{1,2,0:T(2,128)(2,1)S(1)} async-done(((bf16[16,128,1]{1,2,0:T(2,128)(2,1)}), bf16[16,128,1]{1,2,0:T(2,128)(2,1)S(1)}, u32[]{:S(2)}, u32[]{:S(2)}) %all-to-all-start.2) | async-done | bytes 4128 | tf_op jit(solution)/shard_map/all_to_all | solution.py:41
  29.3 3.7 %all-to-all-start.1 = ((bf16[16,256,88]{1,2,0:T(8,128)(2,1)}), bf16[16,256,88]{1,2,0:T(8,128)(2,1)S(1)}, u32[]{:S(2)}, u32[]{:S(2)}) async-start(bf16[16,256,88]{1,2,0:T(8,128)(2,1)} %bitcast.3), calls=%async_computation.1 | async-start | bytes 1441792 | tf_op jit(solution)/shard_map/all_to_all | solution.py:41
  33.1 11.6 %all-to-all-done.1 = bf16[16,256,88]{1,2,0:T(8,128)(2,1)S(1)} async-done(((bf16[16,256,88]{1,2,0:T(8,128)(2,1)}), bf16[16,256,88]{1,2,0:T(8,128)(2,1)S(1)}, u32[]{:S(2)}, u32[]{:S(2)}) %all-to-all-start.1) | async-done | bytes 720928 | tf_op jit(solution)/shard_map/all_to_all | solution.py:41
  45.6 4.3 %all-to-all-start.3 = ((bf16[16,128,88]{1,2,0:T(8,128)(2,1)}), bf16[16,128,88]{1,2,0:T(8,128)(2,1)}, u32[]{:S(2)}, u32[]{:S(2)}) async-start(bf16[16,128,88]{1,2,0:T(8,128)(2,1)} %broadcast_in_dim.21), calls=%async_computation.3 | async-start | bytes 720896 | tf_op jit(solution)/shard_map/all_to_all | solution.py:14
  50.4 7.8 %all-to-all-done.3 = bf16[16,128,88]{1,2,0:T(8,128)(2,1)} async-done(((bf16[16,128,88]{1,2,0:T(8,128)(2,1)}), bf16[16,128,88]{1,2,0:T(8,128)(2,1)}, u32[]{:S(2)}, u32[]{:S(2)}) %all-to-all-start.3) | async-done | bytes 360480 | tf_op jit(solution)/shard_map/all_to_all | solution.py:14
  59.5 11.7 %all_to_all.65 = f32[8,128,32]{1,2,0:T(8,128)S(1)} all-to-all(f32[8,128,32]{1,2,0:T(8,128)S(1)} %convolution_bitcast_fusion.1), channel_id=1, replica_groups=mesh['kv'=16,'tp'=8] {'tp'}, dimensions={0} | all-to-all | bytes 262144 | tf_op jit(solution)/shard_map/all_to_all | solution.py:35
  71.8 4.1 %all-to-all-start.5 = ((bf16[8,128,32]{1,2,0:T(8,128)(2,1)}), bf16[8,128,32]{1,2,0:T(8,128)(2,1)S(1)}, u32[]{:S(2)}, u32[]{:S(2)}) async-start(bf16[8,128,32]{1,2,0:T(8,128)(2,1)} %broadcast_in_dim.22), calls=%async_computation.5 | async-start | bytes 131072 | tf_op jit(solution)/shard_map/all_to_all | solution.py:14
  76.0 4.9 %all-to-all-done.5 = bf16[8,128,32]{1,2,0:T(8,128)(2,1)S(1)} async-done(((bf16[8,128,32]{1,2,0:T(8,128)(2,1)}), bf16[8,128,32]{1,2,0:T(8,128)(2,1)S(1)}, u32[]{:S(2)}, u32[]{:S(2)}) %all-to-all-start.5) | async-done | bytes 65568 | tf_op jit(solution)/shard_map/all_to_all | solution.py:14
  83.9 3.7 %all-to-all-start.6 = ((f32[16,8,2577]{2,1,0:T(8,128)}), f32[16,8,2577]{2,1,0:T(8,128)S(1)}, u32[]{:S(2)}, u32[]{:S(2)}) async-start(f32[16,8,2577]{2,1,0:T(8,128)} %concatenate.23), calls=%async_computation.6 | async-start | bytes 2752512 | tf_op jit(solution)/shard_map/all_to_all | solution.py:35
  87.9 20.5 %all-to-all-done.6 = f32[16,8,2577]{2,1,0:T(8,128)S(1)} async-done(((f32[16,8,2577]{2,1,0:T(8,128)}), f32[16,8,2577]{2,1,0:T(8,128)S(1)}, u32[]{:S(2)}, u32[]{:S(2)}) %all-to-all-start.6) | async-done | bytes 1319456 | tf_op jit(solution)/shard_map/all_to_all | solution.py:35
  109.3 5.3 %multiply_reduce_fusion = (f32[8,16,64]{2,1,0:T(8,128)S(1)}, f32[8,16,64,128]{3,2,1,0:T(8,128)}) fusion(f32[8,16,128]{2,1,0:T(8,128)S(1)} %broadcast_bitcast_fusion, f32[8,16,128]{2,1,0:T(8,128)S(1)} %broadcast_bitcast_fusion.1, f32[8,16,64]{2,1,0:T(8,128)S(1)} %multiply_multiply_fusion, f32[8,16,64,128]{3,2,1,0:T(8,128)} %param.47, ...), kind=kLoop, calls=%fused_computation | loop fusion | flops 5234688 | bytes 8585728 | tf_op jit(solution)/shard_map/reduce_sum | solution.py:133
  114.9 16.0 %all_gather.3 = bf16[128,1024]{1,0:T(8,128)(2,1)S(1)} all-gather(bf16[8,1024]{1,0:T(8,128)(2,1)S(1)} %multiply_convert_fusion.1), channel_id=1, replica_groups=mesh['kv'=16,'tp'=8] {'kv'}, dimensions={0}, use_global_device_ids=true | all-gather | bytes 278528 | tf_op jit(solution)/shard_map/all_gather | solution.py:204
  131.3 15.1 %all_to_all.66 = f32[8,128,32]{1,2,0:T(8,128)S(1)} all-to-all(f32[8,128,32]{1,2,0:T(8,128)S(1)} %bitcast.91), channel_id=1, replica_groups=mesh['kv'=16,'tp'=8] {'tp'}, dimensions={0} | all-to-all | bytes 262144 | tf_op jit(solution)/shard_map/all_to_all | solution.py:35
  147.1 4.1 %all-to-all-start.8 = ((bf16[8,128,32]{1,2,0:T(8,128)(2,1)}), bf16[8,128,32]{1,2,0:T(8,128)(2,1)S(1)}, u32[]{:S(2)}, u32[]{:S(2)}) async-start(bf16[8,128,32]{1,2,0:T(8,128)(2,1)} %broadcast_in_dim.28), calls=%async_computation.8 | async-start | bytes 131072 | tf_op jit(solution)/shard_map/all_to_all | solution.py:14
  151.2 4.9 %all-to-all-done.8 = bf16[8,128,32]{1,2,0:T(8,128)(2,1)S(1)} async-done(((bf16[8,128,32]{1,2,0:T(8,128)(2,1)}), bf16[8,128,32]{1,2,0:T(8,128)(2,1)S(1)}, u32[]{:S(2)}, u32[]{:S(2)}) %all-to-all-start.8) | async-done | bytes 65568 | tf_op jit(solution)/shard_map/all_to_all | solution.py:14
  157.4 4.7 %all-to-all-start.10 = ((bf16[16,128,1]{1,2,0:T(2,128)(2,1)}), bf16[16,128,1]{1,2,0:T(2,128)(2,1)S(1)}, u32[]{:S(2)}, u32[]{:S(2)}) async-start(bf16[16,128,1]{1,2,0:T(2,128)(2,1)} %transpose.97), calls=%async_computation.10 | async-start | bytes 16384 | tf_op jit(solution)/shard_map/all_to_all | solution.py:41
  163.4 5.2 %all-to-all-done.10 = bf16[16,128,1]{1,2,0:T(2,128)(2,1)S(1)} async-done(((bf16[16,128,1]{1,2,0:T(2,128)(2,1)}), bf16[16,128,1]{1,2,0:T(2,128)(2,1)S(1)}, u32[]{:S(2)}, u32[]{:S(2)}) %all-to-all-start.10) | async-done | bytes 4128 | tf_op jit(solution)/shard_map/all_to_all | solution.py:41
  172.2 11.6 %all-to-all-done.9 = bf16[16,256,88]{1,2,0:T(8,128)(2,1)S(1)} async-done(((bf16[16,256,88]{1,2,0:T(8,128)(2,1)}), bf16[16,256,88]{1,2,0:T(8,128)(2,1)S(1)}, u32[]{:S(2)}, u32[]{:S(2)}) %all-to-all-start.9) | async-done | bytes 720928 | tf_op jit(solution)/shard_map/all_to_all | solution.py:41
  188.6 7.7 %all-to-all-done.11 = bf16[16,128,88]{1,2,0:T(8,128)(2,1)S(1)} async-done(((bf16[16,128,88]{1,2,0:T(8,128)(2,1)}), bf16[16,128,88]{1,2,0:T(8,128)(2,1)S(1)}, u32[]{:S(2)}, u32[]{:S(2)}) %all-to-all-start.11) | async-done | bytes 360480 | tf_op jit(solution)/shard_map/all_to_all | solution.py:14
  197.3 7.3 %all-to-all-start.12 = ((f32[8,128,32]{1,2,0:T(8,128)}), f32[8,128,32]{1,2,0:T(8,128)S(1)}, u32[]{:S(2)}, u32[]{:S(2)}) async-start(f32[8,128,32]{1,2,0:T(8,128)} %convolution_bitcast_fusion), calls=%async_computation.12 | async-start | bytes 262144 | tf_op jit(solution)/shard_map/all_to_all | solution.py:35
  205.9 4.0 %all-to-all-done.12 = f32[8,128,32]{1,2,0:T(8,128)S(1)} async-done(((f32[8,128,32]{1,2,0:T(8,128)}), f32[8,128,32]{1,2,0:T(8,128)S(1)}, u32[]{:S(2)}, u32[]{:S(2)}) %all-to-all-start.12) | async-done | bytes 131104 | tf_op jit(solution)/shard_map/all_to_all | solution.py:35
  (133 shorter events, 28.2 us)
Async XLA Ops:
  2.1 10.6 %all-to-all-start = ((bf16[8,128,32]{1,2,0:T(8,128)(2,1)}), bf16[8,128,32]{1,2,0:T(8,128)(2,1)S(1)}, u32[]{:S(2)}, u32[]{:S(2)}) async-start(bf16[8,128,32]{1,2,0:T(8,128)(2,1)} %broadcast_in_dim.20), calls=%async_computation | async-start | bytes 131072 | tf_op jit(solution)/shard_map/all_to_all | solution.py:14
  12.8 37.2 %copy-start.1 = (bf16[1408,256]{1,0:T(8,128)(2,1)S(1)}, bf16[1408,256]{1,0:T(8,128)(2,1)}, u32[]{:S(2)}) copy-start(bf16[1408,256]{1,0:T(8,128)(2,1)} %param.31) | copy-start | bytes 2162692
  15.2 14.1 %all-to-all-start.2 = ((bf16[16,128,1]{1,2,0:T(2,128)(2,1)}), bf16[16,128,1]{1,2,0:T(2,128)(2,1)S(1)}, u32[]{:S(2)}, u32[]{:S(2)}) async-start(bf16[16,128,1]{1,2,0:T(2,128)(2,1)} %transpose.92), calls=%async_computation.2 | async-start | bytes 16384 | tf_op jit(solution)/shard_map/all_to_all | solution.py:41
  23.0 48.1 %copy-start.13 = (bf16[128,32]{0,1:T(8,128)(2,1)S(1)}, bf16[128,32]{0,1:T(8,128)(2,1)}, u32[]{:S(2)}) copy-start(bf16[128,32]{0,1:T(8,128)(2,1)} %param.27) | copy-start | bytes 24580
  23.0 52.9 %copy-start.21 = (bf16[256]{0:T(256)(128)(2,1)S(1)}, bf16[256]{0:T(256)(128)(2,1)}, u32[]{:S(2)}) copy-start(bf16[256]{0:T(256)(128)(2,1)} %param.32) | copy-start | bytes 1540
  29.3 52.0 %copy-start.6 = (bf16[256,1024]{1,0:T(8,128)(2,1)S(1)}, bf16[256,1024]{1,0:T(8,128)(2,1)}, u32[]{:S(2)}) copy-start(bf16[256,1024]{1,0:T(8,128)(2,1)} %param.34) | copy-start | bytes 1572868
  29.3 15.4 %all-to-all-start.1 = ((bf16[16,256,88]{1,2,0:T(8,128)(2,1)}), bf16[16,256,88]{1,2,0:T(8,128)(2,1)S(1)}, u32[]{:S(2)}, u32[]{:S(2)}) async-start(bf16[16,256,88]{1,2,0:T(8,128)(2,1)} %bitcast.3), calls=%async_computation.1 | async-start | bytes 1441792 | tf_op jit(solution)/shard_map/all_to_all | solution.py:41
  33.1 48.5 %copy-start.7 = (bf16[256,1024]{1,0:T(8,128)(2,1)S(1)}, bf16[256,1024]{1,0:T(8,128)(2,1)}, u32[]{:S(2)}) copy-start(bf16[256,1024]{1,0:T(8,128)(2,1)} %param.33) | copy-start | bytes 1572868
  44.8 37.0 %copy-start.9 = (bf16[256,256]{1,0:T(8,128)(2,1)S(1)}, bf16[256,256]{1,0:T(8,128)(2,1)}, u32[]{:S(2)}) copy-start(bf16[256,256]{1,0:T(8,128)(2,1)} %param.36) | copy-start | bytes 393220
  45.6 36.4 %copy-start.10 = (bf16[256,256]{1,0:T(8,128)(2,1)S(1)}, bf16[256,256]{1,0:T(8,128)(2,1)}, u32[]{:S(2)}) copy-start(bf16[256,256]{1,0:T(8,128)(2,1)} %param.35) | copy-start | bytes 393220
  45.6 12.5 %all-to-all-start.3 = ((bf16[16,128,88]{1,2,0:T(8,128)(2,1)}), bf16[16,128,88]{1,2,0:T(8,128)(2,1)}, u32[]{:S(2)}, u32[]{:S(2)}) async-start(bf16[16,128,88]{1,2,0:T(8,128)(2,1)} %broadcast_in_dim.21), calls=%async_computation.3 | async-start | bytes 720896 | tf_op jit(solution)/shard_map/all_to_all | solution.py:14
  50.0 32.3 %copy-start.14 = (bf16[256,16]{0,1:T(8,128)(2,1)S(1)}, bf16[256,16]{0,1:T(8,128)(2,1)}, u32[]{:S(2)}) copy-start(bf16[256,16]{0,1:T(8,128)(2,1)} %param.37) | copy-start | bytes 24580
  71.8 9.0 %all-to-all-start.5 = ((bf16[8,128,32]{1,2,0:T(8,128)(2,1)}), bf16[8,128,32]{1,2,0:T(8,128)(2,1)S(1)}, u32[]{:S(2)}, u32[]{:S(2)}) async-start(bf16[8,128,32]{1,2,0:T(8,128)(2,1)} %broadcast_in_dim.22), calls=%async_computation.5 | async-start | bytes 131072 | tf_op jit(solution)/shard_map/all_to_all | solution.py:14
  81.9 27.1 %copy-start.11 = (bf16[8,3,256]{2,0,1:T(8,128)(2,1)S(1)}, bf16[8,3,256]{2,0,1:T(8,128)(2,1)}, u32[]{:S(2)}) copy-start(bf16[8,3,256]{2,0,1:T(8,128)(2,1)} %param.46) | copy-start | bytes 36868
  83.9 24.5 %all-to-all-start.6 = ((f32[16,8,2577]{2,1,0:T(8,128)}), f32[16,8,2577]{2,1,0:T(8,128)S(1)}, u32[]{:S(2)}, u32[]{:S(2)}) async-start(f32[16,8,2577]{2,1,0:T(8,128)} %concatenate.23), calls=%async_computation.6 | async-start | bytes 2752512 | tf_op jit(solution)/shard_map/all_to_all | solution.py:35
  109.3 41.9 %copy-start.23 = (bf16[256]{0:T(256)(128)(2,1)S(1)}, bf16[256]{0:T(256)(128)(2,1)}, u32[]{:S(2)}) copy-start(bf16[256]{0:T(256)(128)(2,1)} %param.50) | copy-start | bytes 1540
  109.3 46.8 %copy-start.2 = (bf16[256,1408]{1,0:T(8,128)(2,1)S(1)}, bf16[256,1408]{1,0:T(8,128)(2,1)}, u32[]{:S(2)}) copy-start(bf16[256,1408]{1,0:T(8,128)(2,1)} %param.52) | copy-start | bytes 2162692
  109.3 47.2 %copy-start.3 = (bf16[256,1408]{1,0:T(8,128)(2,1)S(1)}, bf16[256,1408]{1,0:T(8,128)(2,1)}, u32[]{:S(2)}) copy-start(bf16[256,1408]{1,0:T(8,128)(2,1)} %param.51) | copy-start | bytes 2162692
  147.1 9.0 %all-to-all-start.8 = ((bf16[8,128,32]{1,2,0:T(8,128)(2,1)}), bf16[8,128,32]{1,2,0:T(8,128)(2,1)S(1)}, u32[]{:S(2)}, u32[]{:S(2)}) async-start(bf16[8,128,32]{1,2,0:T(8,128)(2,1)} %broadcast_in_dim.28), calls=%async_computation.8 | async-start | bytes 131072 | tf_op jit(solution)/shard_map/all_to_all | solution.py:14
  156.2 32.1 %copy-start.4 = (bf16[1408,256]{1,0:T(8,128)(2,1)S(1)}, bf16[1408,256]{1,0:T(8,128)(2,1)}, u32[]{:S(2)}) copy-start(bf16[1408,256]{1,0:T(8,128)(2,1)} %param.53) | copy-start | bytes 2162692
  157.4 11.1 %all-to-all-start.10 = ((bf16[16,128,1]{1,2,0:T(2,128)(2,1)}), bf16[16,128,1]{1,2,0:T(2,128)(2,1)S(1)}, u32[]{:S(2)}, u32[]{:S(2)}) async-start(bf16[16,128,1]{1,2,0:T(2,128)(2,1)} %transpose.97), calls=%async_computation.10 | async-start | bytes 16384 | tf_op jit(solution)/shard_map/all_to_all | solution.py:41
  168.5 15.3 %all-to-all-start.9 = ((bf16[16,256,88]{1,2,0:T(8,128)(2,1)}), bf16[16,256,88]{1,2,0:T(8,128)(2,1)S(1)}, u32[]{:S(2)}, u32[]{:S(2)}) async-start(bf16[16,256,88]{1,2,0:T(8,128)(2,1)} %bitcast.28), calls=%async_computation.9 | async-start | bytes 1441792 | tf_op jit(solution)/shard_map/all_to_all | solution.py:41
  184.7 11.6 %all-to-all-start.11 = ((bf16[16,128,88]{1,2,0:T(8,128)(2,1)}), bf16[16,128,88]{1,2,0:T(8,128)(2,1)S(1)}, u32[]{:S(2)}, u32[]{:S(2)}) async-start(bf16[16,128,88]{1,2,0:T(8,128)(2,1)} %broadcast_in_dim.29), calls=%async_computation.11 | async-start | bytes 720896 | tf_op jit(solution)/shard_map/all_to_all | solution.py:14
  197.3 12.6 %all-to-all-start.12 = ((f32[8,128,32]{1,2,0:T(8,128)}), f32[8,128,32]{1,2,0:T(8,128)S(1)}, u32[]{:S(2)}, u32[]{:S(2)}) async-start(f32[8,128,32]{1,2,0:T(8,128)} %convolution_bitcast_fusion), calls=%async_computation.12 | async-start | bytes 262144 | tf_op jit(solution)/shard_map/all_to_all | solution.py:35
  (11 other events, 153.4 us)
where the time goes:
time: 212 us; the launch traced here: 211 us
  waiting for transfers between devices  87.4 us (41%)
  starting transfers between devices  52.7 us (25%)
  blocking collectives  42.8 us (20%)
  local copies, waits for them, and re-layouts  10.9 us (5%)
  other arithmetic  9.52 us (4%)
  matrix products  5.91 us (3%)
    all_to_all x4, waiting for transfers between devices, sum_at_owner(): lax.all_to_all(blocks, axis, split_axis=0, concat_axis=0, tiled=True)  33.5 us
    all_to_all x5, waiting for transfers between devices, copy_for_each(): return lax.all_to_all(copies, axis, split_axis=0, concat_axis=0, tiled=True)  29.4 us
    all_to_all x2, blocking collectives, sent_and_summed(): lax.all_to_all(in_blocks(shard, dim, length), axis, 0, 0, tiled=True)  26.8 us
    all_to_all x2, waiting for transfers between devices, sent_and_summed(): lax.all_to_all(in_blocks(shard, dim, length), axis, 0, 0, tiled=True)  24.6 us
    all_to_all x5, starting transfers between devices, copy_for_each(): return lax.all_to_all(copies, axis, split_axis=0, concat_axis=0, tiled=True)  21.9 us
    all_to_all x4, starting transfers between devices, sum_at_owner(): lax.all_to_all(blocks, axis, split_axis=0, concat_axis=0, tiled=True)  19.8 us
    all_gather x1, blocking collectives, local(): lax.all_gather(mixer_rows, 'kv', axis=0, tiled=True)  16 us
    all_to_all x2, starting transfers between devices, sent_and_summed(): lax.all_to_all(in_blocks(shard, dim, length), axis, 0, 0, tiled=True)  11 us
  transfers between devices with their start and end apart: 11, of which 11 were waited for; matrix products, arithmetic and copies ran while one was open for 2% of the time, Pallas kernels for 0%

commit v1 on v0

--- a/solution.py
+++ b/solution.py
@@ -7,6 +7,14 @@
 HEAD_DIM = 64
 STATE = 128
 EPS = 1e-06
+
+
+def gather_from_all(array, axis, dim):
+    size = lax.axis_size(axis)
+    repeats = [size if d == dim else 1 for d in range(array.ndim)]
+    return lax.all_to_all(
+        jnp.tile(array, repeats), axis, split_axis=dim, concat_axis=dim, tiled=True
+    )
 
 
 def copy_for_each(shard, axis):
@@ -201,9 +209,7 @@
     )
     mixer_rows = (normed * group_gain.astype(jnp.float32)[None, :]).astype(jnp.bfloat16)
     back_part = jnp.dot(
-        lax.all_gather(mixer_rows, "kv", axis=0, tiled=True),
-        mixer_out,
-        preferred_element_type=jnp.float32,
+        gather_from_all(mixer_rows, "kv", 0), mixer_out, preferred_element_type=jnp.float32
     )
     returned = column_sums(back_part)
     middle = (first_out.astype(jnp.float32) + returned).astype(jnp.bfloat16)

time: 212 us -> 202 us (0.953)
  blocking collectives: 42.8 us -> 21.7 us
  waiting for transfers between devices: 87.4 us -> 94.3 us
  starting transfers between devices: 52.7 us -> 55.7 us
    all_gather x1 -> x0, blocking collectives: 16 us -> none  [local(): lax.all_gather(mixer_rows, 'kv', axis=0, tiled=True)]
    all_to_all x0 -> x1, waiting for transfers between devices: none -> 7.43 us  [gather_from_all(): lax.all_to_all(jnp.tile(array, repeats), axis, split_axis=dim, concat_axi...]
    all_to_all x2, blocking collectives: 26.8 us -> 21.7 us  [sent_and_summed(): lax.all_to_all(in_blocks(shard, dim, length), axis, 0, 0, tiled=True)]
    all_to_all x0 -> x1, starting transfers between devices: none -> 4.36 us  [gather_from_all(): lax.all_to_all(jnp.tile(array, repeats), axis, split_axis=dim, concat_axi...]
  transfers between devices with their start and end apart: 11 -> 12, of which waited for: 11 -> 12; matrix products, arithmetic and copies ran while one was open for 2% -> 3% of each run, Pallas kernels for 0% -> 0%
where the time goes in v1:
time: 202 us; the launch traced here: 201 us
  waiting for transfers between devices  94.3 us (47%)
  starting transfers between devices  55.7 us (28%)
  blocking collectives  21.7 us (11%)
  local copies, waits for them, and re-layouts  11.8 us (6%)
  other arithmetic  10.1 us (5%)
  matrix products  5.87 us (3%)
    all_to_all x4, waiting for transfers between devices, sum_at_owner(): lax.all_to_all(blocks, axis, split_axis=0, concat_axis=0, tiled=True)  33.6 us
    all_to_all x5, waiting for transfers between devices, copy_for_each(): return lax.all_to_all(copies, axis, split_axis=0, concat_axis=0, tiled=True)  28.7 us
    all_to_all x2, waiting for transfers between devices, sent_and_summed(): lax.all_to_all(in_blocks(shard, dim, length), axis, 0, 0, tiled=True)  24.5 us
    all_to_all x5, starting transfers between devices, copy_for_each(): return lax.all_to_all(copies, axis, split_axis=0, concat_axis=0, tiled=True)  21.9 us
    all_to_all x2, blocking collectives, sent_and_summed(): lax.all_to_all(in_blocks(shard, dim, length), axis, 0, 0, tiled=True)  21.7 us
    all_to_all x4, starting transfers between devices, sum_at_owner(): lax.all_to_all(blocks, axis, split_axis=0, concat_axis=0, tiled=True)  18.6 us
    all_to_all x2, starting transfers between devices, sent_and_summed(): lax.all_to_all(in_blocks(shard, dim, length), axis, 0, 0, tiled=True)  10.9 us
    all_to_all x1, waiting for transfers between devices, gather_from_all(): lax.all_to_all(jnp.tile(array, repeats), axis, split_axis=dim, concat_axi...  7.43 us
  transfers between devices with their start and end apart: 12, of which 12 were waited for; matrix products, arithmetic and copies ran while one was open for 3% of the time, Pallas kernels for 0%

profile of v1, /device:TPU:1, one launch (start us, length us, event | category | flops | bytes accessed | tf_op | source)
XLA Modules:
  0.0 200.8 jit_solution(9271830879235140457)
XLA Ops:
  2.1 5.8 %all-to-all-start = ((bf16[8,128,32]{1,2,0:T(8,128)(2,1)}), bf16[8,128,32]{1,2,0:T(8,128)(2,1)S(1)}, u32[]{:S(2)}, u32[]{:S(2)}) async-start(bf16[8,128,32]{1,2,0:T(8,128)(2,1)} %broadcast_in_dim.20), calls=%async_computation | async-start | bytes 131072 | tf_op jit(solution)/shard_map/all_to_all | solution.py:22
  8.5 4.2 %all-to-all-done = bf16[8,128,32]{1,2,0:T(8,128)(2,1)S(1)} async-done(((bf16[8,128,32]{1,2,0:T(8,128)(2,1)}), bf16[8,128,32]{1,2,0:T(8,128)(2,1)S(1)}, u32[]{:S(2)}, u32[]{:S(2)}) %all-to-all-start) | async-done | bytes 65568 | tf_op jit(solution)/shard_map/all_to_all | solution.py:22
  15.2 7.8 %all-to-all-start.2 = ((bf16[16,128,1]{1,2,0:T(2,128)(2,1)}), bf16[16,128,1]{1,2,0:T(2,128)(2,1)S(1)}, u32[]{:S(2)}, u32[]{:S(2)}) async-start(bf16[16,128,1]{1,2,0:T(2,128)(2,1)} %transpose.94), calls=%async_computation.2 | async-start | bytes 16384 | tf_op jit(solution)/shard_map/all_to_all | solution.py:49
  24.2 5.1 %all-to-all-done.2 = bf16[16,128,1]{1,2,0:T(2,128)(2,1)S(1)} async-done(((bf16[16,128,1]{1,2,0:T(2,128)(2,1)}), bf16[16,128,1]{1,2,0:T(2,128)(2,1)S(1)}, u32[]{:S(2)}, u32[]{:S(2)}) %all-to-all-start.2) | async-done | bytes 4128 | tf_op jit(solution)/shard_map/all_to_all | solution.py:49
  29.3 3.7 %all-to-all-start.1 = ((bf16[16,256,88]{1,2,0:T(8,128)(2,1)}), bf16[16,256,88]{1,2,0:T(8,128)(2,1)S(1)}, u32[]{:S(2)}, u32[]{:S(2)}) async-start(bf16[16,256,88]{1,2,0:T(8,128)(2,1)} %bitcast.3), calls=%async_computation.1 | async-start | bytes 1441792 | tf_op jit(solution)/shard_map/all_to_all | solution.py:49
  33.1 11.6 %all-to-all-done.1 = bf16[16,256,88]{1,2,0:T(8,128)(2,1)S(1)} async-done(((bf16[16,256,88]{1,2,0:T(8,128)(2,1)}), bf16[16,256,88]{1,2,0:T(8,128)(2,1)S(1)}, u32[]{:S(2)}, u32[]{:S(2)}) %all-to-all-start.1) | async-done | bytes 720928 | tf_op jit(solution)/shard_map/all_to_all | solution.py:49
  45.7 4.3 %all-to-all-start.3 = ((bf16[16,128,88]{1,2,0:T(8,128)(2,1)}), bf16[16,128,88]{1,2,0:T(8,128)(2,1)}, u32[]{:S(2)}, u32[]{:S(2)}) async-start(bf16[16,128,88]{1,2,0:T(8,128)(2,1)} %broadcast_in_dim.21), calls=%async_computation.3 | async-start | bytes 720896 | tf_op jit(solution)/shard_map/all_to_all | solution.py:22
  50.4 7.8 %all-to-all-done.3 = bf16[16,128,88]{1,2,0:T(8,128)(2,1)} async-done(((bf16[16,128,88]{1,2,0:T(8,128)(2,1)}), bf16[16,128,88]{1,2,0:T(8,128)(2,1)}, u32[]{:S(2)}, u32[]{:S(2)}) %all-to-all-start.3) | async-done | bytes 360480 | tf_op jit(solution)/shard_map/all_to_all | solution.py:22
  59.5 11.7 %all_to_all.74 = f32[8,128,32]{1,2,0:T(8,128)S(1)} all-to-all(f32[8,128,32]{1,2,0:T(8,128)S(1)} %convolution_bitcast_fusion.2), channel_id=1, replica_groups=mesh['kv'=16,'tp'=8] {'tp'}, dimensions={0} | all-to-all | bytes 262144 | tf_op jit(solution)/shard_map/all_to_all | solution.py:43
  71.8 4.1 %all-to-all-start.5 = ((bf16[8,128,32]{1,2,0:T(8,128)(2,1)}), bf16[8,128,32]{1,2,0:T(8,128)(2,1)S(1)}, u32[]{:S(2)}, u32[]{:S(2)}) async-start(bf16[8,128,32]{1,2,0:T(8,128)(2,1)} %broadcast_in_dim.22), calls=%async_computation.5 | async-start | bytes 131072 | tf_op jit(solution)/shard_map/all_to_all | solution.py:22
  76.0 4.9 %all-to-all-done.5 = bf16[8,128,32]{1,2,0:T(8,128)(2,1)S(1)} async-done(((bf16[8,128,32]{1,2,0:T(8,128)(2,1)}), bf16[8,128,32]{1,2,0:T(8,128)(2,1)S(1)}, u32[]{:S(2)}, u32[]{:S(2)}) %all-to-all-start.5) | async-done | bytes 65568 | tf_op jit(solution)/shard_map/all_to_all | solution.py:22
  84.0 3.7 %all-to-all-start.6 = ((f32[16,8,2577]{2,1,0:T(8,128)}), f32[16,8,2577]{2,1,0:T(8,128)S(1)}, u32[]{:S(2)}, u32[]{:S(2)}) async-start(f32[16,8,2577]{2,1,0:T(8,128)} %concatenate.23), calls=%async_computation.6 | async-start | bytes 2752512 | tf_op jit(solution)/shard_map/all_to_all | solution.py:43
  87.9 20.5 %all-to-all-done.6 = f32[16,8,2577]{2,1,0:T(8,128)S(1)} async-done(((f32[16,8,2577]{2,1,0:T(8,128)}), f32[16,8,2577]{2,1,0:T(8,128)S(1)}, u32[]{:S(2)}, u32[]{:S(2)}) %all-to-all-start.6) | async-done | bytes 1319456 | tf_op jit(solution)/shard_map/all_to_all | solution.py:43
  109.3 5.2 %multiply_reduce_fusion = (f32[8,16,64]{2,1,0:T(8,128)S(1)}, f32[8,16,64,128]{3,2,1,0:T(8,128)}) fusion(f32[8,16,128]{2,1,0:T(8,128)S(1)} %broadcast_bitcast_fusion, f32[8,16,128]{2,1,0:T(8,128)S(1)} %broadcast_bitcast_fusion.1, f32[8,16,64]{2,1,0:T(8,128)S(1)} %multiply_multiply_fusion, f32[8,16,64,128]{3,2,1,0:T(8,128)} %param.47, ...), kind=kLoop, calls=%fused_computation | loop fusion | flops 5234688 | bytes 8585728 | tf_op jit(solution)/shard_map/reduce_sum | solution.py:141
  115.6 4.4 %all-to-all-start.7 = ((bf16[16,8,1024]{2,1,0:T(8,128)(2,1)}), bf16[16,8,1024]{2,1,0:T(8,128)(2,1)S(1)}, u32[]{:S(2)}, u32[]{:S(2)}) async-start(bf16[16,8,1024]{2,1,0:T(8,128)(2,1)} %tile.2), calls=%async_computation.7 | async-start | bytes 524288 | tf_op jit(solution)/shard_map/all_to_all | solution.py:15
  120.2 7.4 %all-to-all-done.7 = bf16[16,8,1024]{2,1,0:T(8,128)(2,1)S(1)} async-done(((bf16[16,8,1024]{2,1,0:T(8,128)(2,1)}), bf16[16,8,1024]{2,1,0:T(8,128)(2,1)S(1)}, u32[]{:S(2)}, u32[]{:S(2)}) %all-to-all-start.7) | async-done | bytes 262176 | tf_op jit(solution)/shard_map/all_to_all | solution.py:15
  127.9 10.0 %all_to_all.75 = f32[8,128,32]{1,2,0:T(8,128)S(1)} all-to-all(f32[8,128,32]{1,2,0:T(8,128)S(1)} %convolution_bitcast_fusion.1), channel_id=1, replica_groups=mesh['kv'=16,'tp'=8] {'tp'}, dimensions={0} | all-to-all | bytes 262144 | tf_op jit(solution)/shard_map/all_to_all | solution.py:43
  138.6 4.1 %all-to-all-start.9 = ((bf16[8,128,32]{1,2,0:T(8,128)(2,1)}), bf16[8,128,32]{1,2,0:T(8,128)(2,1)S(1)}, u32[]{:S(2)}, u32[]{:S(2)}) async-start(bf16[8,128,32]{1,2,0:T(8,128)(2,1)} %broadcast_in_dim.28), calls=%async_computation.9 | async-start | bytes 131072 | tf_op jit(solution)/shard_map/all_to_all | solution.py:22
  143.4 4.2 %all-to-all-done.9 = bf16[8,128,32]{1,2,0:T(8,128)(2,1)S(1)} async-done(((bf16[8,128,32]{1,2,0:T(8,128)(2,1)}), bf16[8,128,32]{1,2,0:T(8,128)(2,1)S(1)}, u32[]{:S(2)}, u32[]{:S(2)}) %all-to-all-start.9) | async-done | bytes 65568 | tf_op jit(solution)/shard_map/all_to_all | solution.py:22
  153.7 5.1 %all-to-all-done.11 = bf16[16,128,1]{1,2,0:T(2,128)(2,1)S(1)} async-done(((bf16[16,128,1]{1,2,0:T(2,128)(2,1)}), bf16[16,128,1]{1,2,0:T(2,128)(2,1)S(1)}, u32[]{:S(2)}, u32[]{:S(2)}) %all-to-all-start.11) | async-done | bytes 4128 | tf_op jit(solution)/shard_map/all_to_all | solution.py:49
  162.5 11.8 %all-to-all-done.10 = bf16[16,256,88]{1,2,0:T(8,128)(2,1)S(1)} async-done(((bf16[16,256,88]{1,2,0:T(8,128)(2,1)}), bf16[16,256,88]{1,2,0:T(8,128)(2,1)S(1)}, u32[]{:S(2)}, u32[]{:S(2)}) %all-to-all-start.10) | async-done | bytes 720928 | tf_op jit(solution)/shard_map/all_to_all | solution.py:49
  179.1 7.7 %all-to-all-done.12 = bf16[16,128,88]{1,2,0:T(8,128)(2,1)S(1)} async-done(((bf16[16,128,88]{1,2,0:T(8,128)(2,1)}), bf16[16,128,88]{1,2,0:T(8,128)(2,1)S(1)}, u32[]{:S(2)}, u32[]{:S(2)}) %all-to-all-start.12) | async-done | bytes 360480 | tf_op jit(solution)/shard_map/all_to_all | solution.py:22
  187.8 7.2 %all-to-all-start.13 = ((f32[8,128,32]{1,2,0:T(8,128)}), f32[8,128,32]{1,2,0:T(8,128)S(1)}, u32[]{:S(2)}, u32[]{:S(2)}) async-start(f32[8,128,32]{1,2,0:T(8,128)} %convolution_bitcast_fusion), calls=%async_computation.13 | async-start | bytes 262144 | tf_op jit(solution)/shard_map/all_to_all | solution.py:43
  196.2 4.0 %all-to-all-done.13 = f32[8,128,32]{1,2,0:T(8,128)S(1)} async-done(((f32[8,128,32]{1,2,0:T(8,128)}), f32[8,128,32]{1,2,0:T(8,128)S(1)}, u32[]{:S(2)}, u32[]{:S(2)}) %all-to-all-start.13) | async-done | bytes 131104 | tf_op jit(solution)/shard_map/all_to_all | solution.py:43
  (138 shorter events, 33.2 us)
Async XLA Ops:
  2.1 10.6 %all-to-all-start = ((bf16[8,128,32]{1,2,0:T(8,128)(2,1)}), bf16[8,128,32]{1,2,0:T(8,128)(2,1)S(1)}, u32[]{:S(2)}, u32[]{:S(2)}) async-start(bf16[8,128,32]{1,2,0:T(8,128)(2,1)} %broadcast_in_dim.20), calls=%async_computation | async-start | bytes 131072 | tf_op jit(solution)/shard_map/all_to_all | solution.py:22
  12.8 37.2 %copy-start.1 = (bf16[1408,256]{1,0:T(8,128)(2,1)S(1)}, bf16[1408,256]{1,0:T(8,128)(2,1)}, u32[]{:S(2)}) copy-start(bf16[1408,256]{1,0:T(8,128)(2,1)} %param.31) | copy-start | bytes 2162692
  15.2 14.1 %all-to-all-start.2 = ((bf16[16,128,1]{1,2,0:T(2,128)(2,1)}), bf16[16,128,1]{1,2,0:T(2,128)(2,1)S(1)}, u32[]{:S(2)}, u32[]{:S(2)}) async-start(bf16[16,128,1]{1,2,0:T(2,128)(2,1)} %transpose.94), calls=%async_computation.2 | async-start | bytes 16384 | tf_op jit(solution)/shard_map/all_to_all | solution.py:49
  23.0 48.1 %copy-start.15 = (bf16[128,32]{0,1:T(8,128)(2,1)S(1)}, bf16[128,32]{0,1:T(8,128)(2,1)}, u32[]{:S(2)}) copy-start(bf16[128,32]{0,1:T(8,128)(2,1)} %param.27) | copy-start | bytes 24580
  23.1 52.9 %copy-start.23 = (bf16[256]{0:T(256)(128)(2,1)S(1)}, bf16[256]{0:T(256)(128)(2,1)}, u32[]{:S(2)}) copy-start(bf16[256]{0:T(256)(128)(2,1)} %param.32) | copy-start | bytes 1540
  29.3 52.0 %copy-start.5 = (bf16[256,1024]{1,0:T(8,128)(2,1)S(1)}, bf16[256,1024]{1,0:T(8,128)(2,1)}, u32[]{:S(2)}) copy-start(bf16[256,1024]{1,0:T(8,128)(2,1)} %param.34) | copy-start | bytes 1572868
  29.3 15.4 %all-to-all-start.1 = ((bf16[16,256,88]{1,2,0:T(8,128)(2,1)}), bf16[16,256,88]{1,2,0:T(8,128)(2,1)S(1)}, u32[]{:S(2)}, u32[]{:S(2)}) async-start(bf16[16,256,88]{1,2,0:T(8,128)(2,1)} %bitcast.3), calls=%async_computation.1 | async-start | bytes 1441792 | tf_op jit(solution)/shard_map/all_to_all | solution.py:49
  33.1 48.5 %copy-start.6 = (bf16[256,1024]{1,0:T(8,128)(2,1)S(1)}, bf16[256,1024]{1,0:T(8,128)(2,1)}, u32[]{:S(2)}) copy-start(bf16[256,1024]{1,0:T(8,128)(2,1)} %param.33) | copy-start | bytes 1572868
  44.9 37.0 %copy-start.9 = (bf16[256,256]{1,0:T(8,128)(2,1)S(1)}, bf16[256,256]{1,0:T(8,128)(2,1)}, u32[]{:S(2)}) copy-start(bf16[256,256]{1,0:T(8,128)(2,1)} %param.35) | copy-start | bytes 393220
  45.7 36.4 %copy-start.10 = (bf16[256,256]{1,0:T(8,128)(2,1)S(1)}, bf16[256,256]{1,0:T(8,128)(2,1)}, u32[]{:S(2)}) copy-start(bf16[256,256]{1,0:T(8,128)(2,1)} %param.36) | copy-start | bytes 393220
  45.7 12.5 %all-to-all-start.3 = ((bf16[16,128,88]{1,2,0:T(8,128)(2,1)}), bf16[16,128,88]{1,2,0:T(8,128)(2,1)}, u32[]{:S(2)}, u32[]{:S(2)}) async-start(bf16[16,128,88]{1,2,0:T(8,128)(2,1)} %broadcast_in_dim.21), calls=%async_computation.3 | async-start | bytes 720896 | tf_op jit(solution)/shard_map/all_to_all | solution.py:22
  50.0 32.3 %copy-start.16 = (bf16[256,16]{0,1:T(8,128)(2,1)S(1)}, bf16[256,16]{0,1:T(8,128)(2,1)}, u32[]{:S(2)}) copy-start(bf16[256,16]{0,1:T(8,128)(2,1)} %param.37) | copy-start | bytes 24580
  71.8 9.0 %all-to-all-start.5 = ((bf16[8,128,32]{1,2,0:T(8,128)(2,1)}), bf16[8,128,32]{1,2,0:T(8,128)(2,1)S(1)}, u32[]{:S(2)}, u32[]{:S(2)}) async-start(bf16[8,128,32]{1,2,0:T(8,128)(2,1)} %broadcast_in_dim.22), calls=%async_computation.5 | async-start | bytes 131072 | tf_op jit(solution)/shard_map/all_to_all | solution.py:22
  84.0 24.5 %all-to-all-start.6 = ((f32[16,8,2577]{2,1,0:T(8,128)}), f32[16,8,2577]{2,1,0:T(8,128)S(1)}, u32[]{:S(2)}, u32[]{:S(2)}) async-start(f32[16,8,2577]{2,1,0:T(8,128)} %concatenate.23), calls=%async_computation.6 | async-start | bytes 2752512 | tf_op jit(solution)/shard_map/all_to_all | solution.py:43
  109.3 38.4 %copy-start.2 = (bf16[256,1408]{1,0:T(8,128)(2,1)S(1)}, bf16[256,1408]{1,0:T(8,128)(2,1)}, u32[]{:S(2)}) copy-start(bf16[256,1408]{1,0:T(8,128)(2,1)} %param.52) | copy-start | bytes 2162692
  114.5 33.5 %copy-start.3 = (bf16[256,1408]{1,0:T(8,128)(2,1)S(1)}, bf16[256,1408]{1,0:T(8,128)(2,1)}, u32[]{:S(2)}) copy-start(bf16[256,1408]{1,0:T(8,128)(2,1)} %param.51) | copy-start | bytes 2162692
  115.6 12.0 %all-to-all-start.7 = ((bf16[16,8,1024]{2,1,0:T(8,128)(2,1)}), bf16[16,8,1024]{2,1,0:T(8,128)(2,1)S(1)}, u32[]{:S(2)}, u32[]{:S(2)}) async-start(bf16[16,8,1024]{2,1,0:T(8,128)(2,1)} %tile.2), calls=%async_computation.7 | async-start | bytes 524288 | tf_op jit(solution)/shard_map/all_to_all | solution.py:15
  138.6 9.0 %all-to-all-start.9 = ((bf16[8,128,32]{1,2,0:T(8,128)(2,1)}), bf16[8,128,32]{1,2,0:T(8,128)(2,1)S(1)}, u32[]{:S(2)}, u32[]{:S(2)}) async-start(bf16[8,128,32]{1,2,0:T(8,128)(2,1)} %broadcast_in_dim.28), calls=%async_computation.9 | async-start | bytes 131072 | tf_op jit(solution)/shard_map/all_to_all | solution.py:22
  149.0 9.8 %all-to-all-start.11 = ((bf16[16,128,1]{1,2,0:T(2,128)(2,1)}), bf16[16,128,1]{1,2,0:T(2,128)(2,1)S(1)}, u32[]{:S(2)}, u32[]{:S(2)}) async-start(bf16[16,128,1]{1,2,0:T(2,128)(2,1)} %transpose.99), calls=%async_computation.11 | async-start | bytes 16384 | tf_op jit(solution)/shard_map/all_to_all | solution.py:49
  152.6 42.4 %copy-start.12 = (bf16[8,3,256]{2,0,1:T(8,128)(2,1)S(1)}, bf16[8,3,256]{2,0,1:T(8,128)(2,1)}, u32[]{:S(2)}) copy-start(bf16[8,3,256]{2,0,1:T(8,128)(2,1)} %param.46) | copy-start | bytes 36868
  152.6 42.3 %copy-start.14 = (bf16[8,3,256]{2,0,1:T(8,128)(2,1)S(1)}, bf16[8,3,256]{2,0,1:T(8,128)(2,1)}, u32[]{:S(2)}) copy-start(bf16[8,3,256]{2,0,1:T(8,128)(2,1)} %param.45) | copy-start | bytes 36868
  158.8 15.4 %all-to-all-start.10 = ((bf16[16,256,88]{1,2,0:T(8,128)(2,1)}), bf16[16,256,88]{1,2,0:T(8,128)(2,1)S(1)}, u32[]{:S(2)}, u32[]{:S(2)}) async-start(bf16[16,256,88]{1,2,0:T(8,128)(2,1)} %bitcast.31), calls=%async_computation.10 | async-start | bytes 1441792 | tf_op jit(solution)/shard_map/all_to_all | solution.py:49
  175.2 11.6 %all-to-all-start.12 = ((bf16[16,128,88]{1,2,0:T(8,128)(2,1)}), bf16[16,128,88]{1,2,0:T(8,128)(2,1)S(1)}, u32[]{:S(2)}, u32[]{:S(2)}) async-start(bf16[16,128,88]{1,2,0:T(8,128)(2,1)} %broadcast_in_dim.29), calls=%async_computation.12 | async-start | bytes 720896 | tf_op jit(solution)/shard_map/all_to_all | solution.py:22
  187.8 12.4 %all-to-all-start.13 = ((f32[8,128,32]{1,2,0:T(8,128)}), f32[8,128,32]{1,2,0:T(8,128)S(1)}, u32[]{:S(2)}, u32[]{:S(2)}) async-start(f32[8,128,32]{1,2,0:T(8,128)} %convolution_bitcast_fusion), calls=%async_computation.13 | async-start | bytes 262144 | tf_op jit(solution)/shard_map/all_to_all | solution.py:43
  (13 other events, 199.7 us)
